TPU v7x, 32 devices: a whole 2x2x4 slice. The times are simulated.
32 devices in a mesh: sp: 8 (over z, y), tp: 4 (over x, core).
Axes of the slice: x: 2, y: 2, z: 4, core: 2. Of those that a mesh axis runs over, the one named last changes fastest.
Arguments:
- stream: bfloat16 [2048, 2048], P('sp'), may hold values from -6 to 6
- attn_gain: float32 [2, 2048], replicated, may hold values from 0.1 to 1.9
- w_query: bfloat16 [2, 2048, 2048], P(None, None, 'tp'), may hold values from -0.125 to 0.125
- w_key: bfloat16 [2, 2048, 512], P(None, None, 'tp'), may hold values from -0.125 to 0.125
- w_value: bfloat16 [2, 2048, 512], P(None, None, 'tp'), may hold values from -0.125 to 0.125
- w_out: bfloat16 [2, 2048, 2048], P(None, 'tp'), may hold values from -1 to 1
- query_gain: float32 [2, 64], replicated, may hold values from 0.1 to 1.9
- key_gain: float32 [2, 64], replicated, may hold values from 0.1 to 1.9
- rel_bias: float32 [2, 32, 257], P(None, 'tp'), may hold values from -6 to 300
Outputs:
- result: bfloat16 [2048, 2048], P('sp', 'tp')
All inputs are finite; a program needn't handle non-finite values.
Results may differ from a plain program's by a relative error of at most 0.02.
Values may be sent and summed in bfloat16 or wider, within the bound.
A program may use at most 64 MiB of HBM per device.

v0:
```python
import jax
import jax.numpy as jnp
from jax import lax
from jax.sharding import PartitionSpec as P

HEAD_DIM = 64
SEG = 64
LEFT = 4
CLIP = 128
LAYERS = 2


norm_eps = 1e-06
masked_score = -1e30


def passed_along(value, axis, steps):
    count = lax.axis_size(axis)
    initial, last = (max(0, -steps), min(count, count - steps))
    return lax.ppermute(value, axis, [(source, source + steps) for source in range(initial, last)])


def rms_scale(values_in, gain):
    squared = jnp.mean(values_in * values_in, axis=-1, keepdims=True)
    return values_in * lax.rsqrt(squared + norm_eps) * gain


def segment_bias(bias_table, span):
    line_len = SEG + span - 1
    offset = jnp.arange(line_len, dtype=jnp.int32)
    distance = jnp.clip(LEFT * SEG + SEG - 1 - offset, -CLIP, CLIP) + CLIP
    table_cols = jnp.arange(bias_table.shape[1], dtype=jnp.int32)
    onehot = (table_cols[:, None] == distance[None, :]).astype(jnp.float32)
    line = jnp.dot(
        bias_table, onehot, precision=lax.Precision.HIGHEST, preferred_element_type=jnp.float32
    )
    rows = [line[:, SEG - 1 - q : SEG - 1 - q + span] for q in range(SEG)]
    return jnp.stack(rows, axis=1)


def project_pair(normed, key_weight, value_weight, key_gain_row):
    row_count = normed.shape[0]
    key_flat = jnp.dot(normed, key_weight, preferred_element_type=jnp.float32)
    keys_made = (
        rms_scale(key_flat.reshape(row_count, -1, HEAD_DIM), key_gain_row)
        .astype(jnp.bfloat16)
        .reshape(row_count, -1)
    )
    values_made = jnp.dot(normed, value_weight, preferred_element_type=jnp.float32).astype(
        jnp.bfloat16
    )
    return (keys_made, values_made)


def band_attention(queries, keys_all, values_all, bias_table, first_pos):
    key_reach = LEFT * SEG
    span = (LEFT + 1) * SEG
    row_count = queries.shape[0]
    kv_here = keys_all.shape[1] // HEAD_DIM
    heads_here = queries.shape[1] // HEAD_DIM
    group = heads_here // kv_here
    bias = segment_bias(bias_table, span).reshape(kv_here, group, 1, SEG, span)
    seg_index = jnp.arange(LEFT, dtype=jnp.int32)[:, None]
    key_index = jnp.arange(span, dtype=jnp.int32)[None, :]

    def one_block(block_index):
        start = block_index * key_reach
        query_rows = queries.reshape(LEFT, SEG, kv_here, group, HEAD_DIM)
        key_rows = keys_all.reshape(2 * key_reach, kv_here, HEAD_DIM)
        value_rows = values_all.reshape(2 * key_reach, kv_here, HEAD_DIM)
        key_windows = jnp.stack([key_rows[q * SEG : q * SEG + span] for q in range(LEFT)], axis=0)
        value_windows = jnp.stack(
            [value_rows[q * SEG : q * SEG + span] for q in range(LEFT)], axis=0
        )
        scores = (
            jnp.einsum(
                "nqkgd,njkd->kgnqj", query_rows, key_windows, preferred_element_type=jnp.float32
            )
            * HEAD_DIM ** (-0.5)
            + bias
        )
        inside = first_pos + start + (seg_index - LEFT) * SEG + key_index >= 0
        scores = jnp.where(inside[None, None, :, None, :], scores, masked_score)
        peak = jnp.max(scores, axis=-1, keepdims=True)
        expon = jnp.exp(scores - peak)
        weights = (expon / jnp.sum(expon, axis=-1, keepdims=True)).astype(jnp.bfloat16)
        mixed = jnp.einsum(
            "kgnqj,njkd->nqkgd", weights, value_windows, preferred_element_type=jnp.float32
        )
        return mixed.astype(jnp.bfloat16).reshape(key_reach, heads_here * HEAD_DIM)

    blocks = lax.map(one_block, jnp.arange(row_count // key_reach, dtype=jnp.int32))
    return blocks.reshape(row_count, heads_here * HEAD_DIM)


def local(stream, attn_gain, w_query, w_key, w_value, w_out, query_gain, key_gain, rel_bias):
    row_count = stream.shape[0]
    key_reach = LEFT * SEG
    first_pos = lax.axis_index("sp") * row_count
    current = stream
    for layer_index in range(LAYERS):
        normed = rms_scale(current.astype(jnp.float32), attn_gain[layer_index]).astype(jnp.bfloat16)
        query_flat = jnp.dot(normed, w_query[layer_index], preferred_element_type=jnp.float32)
        queries = (
            rms_scale(query_flat.reshape(row_count, -1, HEAD_DIM), query_gain[layer_index])
            .astype(jnp.bfloat16)
            .reshape(row_count, -1)
        )
        keys_now, values_now = project_pair(
            normed, w_key[layer_index], w_value[layer_index], key_gain[layer_index]
        )
        rows_prior = passed_along(normed, "sp", 1)
        keys_prior, values_prior = project_pair(
            rows_prior, w_key[layer_index], w_value[layer_index], key_gain[layer_index]
        )
        keys_all = jnp.concatenate([keys_prior, keys_now], axis=0)
        values_all = jnp.concatenate([values_prior, values_now], axis=0)
        mixed = band_attention(queries, keys_all, values_all, rel_bias[layer_index], first_pos)
        partial_value = jnp.dot(mixed, w_out[layer_index], preferred_element_type=jnp.float32)
        if layer_index < LAYERS - 1:
            summed = lax.psum(partial_value.astype(jnp.bfloat16), "tp").astype(jnp.float32)
            current = (current.astype(jnp.float32) + summed).astype(jnp.bfloat16)
        else:
            summed = lax.psum_scatter(
                partial_value.astype(jnp.bfloat16), "tp", scatter_dimension=1, tiled=True
            ).astype(jnp.float32)
            feature_cols = summed.shape[1]
            own_cols = lax.dynamic_slice_in_dim(
                current, lax.axis_index("tp") * feature_cols, feature_cols, 1
            )
            current = (own_cols.astype(jnp.float32) + summed).astype(jnp.bfloat16)
    return current


def solution(mesh):
    return jax.shard_map(
        local,
        mesh=mesh,
        in_specs=(
            P("sp", None),
            P(),
            P(None, None, "tp"),
            P(None, None, "tp"),
            P(None, None, "tp"),
            P(None, "tp", None),
            P(),
            P(),
            P(None, "tp", None),
        ),
        out_specs=P("sp", "tp"),
        check_vma=False,
    )
```

profile of v0, /device:TPU:0, one launch (start us, length us, event | category | flops | bytes accessed | tf_op | source)
XLA Modules:
  0.0 247.3 jit_solution(2282217195734289427)
XLA Ops:
  9.5 2.5 %fusion.13 = bf16[256,2048]{1,0:T(8,128)(2,1)} fusion(bf16[256,2048]{1,0:T(8,128)(2,1)} %param.9, f32[2048]{0:T(1024)S(1)} %bitcast.209, f32[256]{0:T(256)S(1)} %add_rsqrt_fusion.7), kind=kLoop, calls=%fused_computation.24 | loop fusion | flops 2097152 | bytes 2106368 | tf_op jit(solution)/shard_map/convert_element_type | solution.py:102
  12.0 5.9 %collective-permute-start = (bf16[256,2048]{1,0:T(8,128)(2,1)}, bf16[256,2048]{1,0:T(8,128)(2,1)}, u32[]{:S(2)}, u32[]{:S(2)}) collective-permute-start(bf16[256,2048]{1,0:T(8,128)(2,1)} %fusion.13), channel_id=1, source_target_pairs={{0,4},{4,8},{8,12},{12,16},{16,20},{20,24},{24,28},{1,5},{5,9},{9,... | collective-permute-start | bytes 3145736 | tf_op jit(solution)/shard_map/ppermute | solution.py:20
  21.2 3.8 %slice_bitcast_fusion.1 = (bf16[512,2048]{0,1:T(8,128)(2,1)}, bf16[512,2048]{0,1:T(8,128)(2,1)S(1)}) fusion(bf16[2,2048,512]{2,1,0:T(8,128)(2,1)} %param.11), kind=kLoop, calls=%fused_computation.31 | loop fusion | bytes 8388608 | tf_op jit(solution)/shard_map/dot_general | solution.py:103
  25.1 4.0 %copy.159 = bf16[512,2048]{1,0:T(8,128)(2,1)} copy(bf16[512,2048]{0,1:T(8,128)(2,1)} %get-tuple-element.41) | data formatting | bytes 4194304 | tf_op jit(solution)/shard_map/dot_general | solution.py:103
  29.0 3.5 %multiply_reduce_fusion.1 = (f32[256,8]{0,1:T(8,128)S(1)}, f32[256,8,64]{0,2,1:T(8,128)}) fusion(bf16[8,64,2048]{2,1,0:T(8,128)(2,1)} %bitcast.185, bf16[256,2048]{1,0:T(8,128)(2,1)} %fusion.13), kind=kOutput, calls=%fused_computation.79 | convolution fusion | flops 537131008 | bytes 3678208 | tf_op jit(solution)/shard_map/dot_general | solution.py:103
  35.0 1.8 multiply_reduce_fusion.4
  96.6 7.7 %stack.544 = f32[2,4,1,64,320]{4,3,1,0,2:T(8,128)S(1)} concatenate(f32[2,4,1,1,320]{4,3,1,0,2:T(1,128)} %stack.620, f32[2,4,1,1,320]{4,3,1,0,2:T(1,128)} %stack.621, f32[2,4,1,1,320]{4,3,1,0,2:T(1,128)} %stack.622, f32[2,4,1,1,320]{4,3,1,0,2:T(1,128)} %stack.623, f32[2,4,1,1,320]{4,3,1,0,2:T(1,128)} %stack.624, f32[2,4,1,1,320]{4,3,1,0,2:T(1,128)} %stack.625, ...), dimensions={3} | concatenate | bytes 1310720 | tf_op jit(solution)/shard_map/stack | solution.py:38
  106.7 1.8 convolution_convert_fusion.4
  117.5 1.7 multiply_reduce_fusion.5
  120.2 4.1 %fusion.143 = (f32[2,4,4,64]{3,1,2,0:T(4,128)S(1)}, f32[2,4,4,64,320]{4,3,1,2,0:T(8,128)}) fusion(f32[2,4,64,320]{3,2,1,0:T(8,128)S(1)} %bitcast.187, pred[4,320]{1,0:T(4,128)(4,1)} %add_compare_fusion, bf16[4,64,2,4,64]{1,0,4,3,2:T(4,128)(2,1)} %reshape_reshape.8, bf16[1,320,2,64]{1,3,0,2:T(8,128)(2,1)S(1)} %bitcast.198, ...), kind=kOutput, calls=%fused_computation.202 | convolution fusion | flops 88473920 | bytes 3876096 | tf_op jit(solution)/shard_map/while/body/eval_jaxpr/sub | solution.py:85
  124.3 3.2 %fusion.40 = bf16[4,64,2,4,64]{1,4,3,2,0:T(8,128)(2,1)S(1)} fusion(bf16[1,320,2,64]{1,3,2,0:T(8,128)(2,1)S(1)} %bitcast.202, bf16[1,320,2,64]{1,3,2,0:T(8,128)(2,1)S(1)} %bitcast.204, bf16[1,320,2,64]{1,3,2,0:T(8,128)(2,1)} %bitcast.205, bf16[1,320,2,64]{1,3,2,0:T(8,128)(2,1)} %bitcast.207, f32[2,4,4,64,320]{4,3,1,2,0:T(8,128)} %get-tuple-element.226, ...), kind=kOutput, calls=%fused_computation.47 | convolution fusion | flops 86638592 | bytes 3219456 | tf_op jit(solution)/shard_map/while/body/eval_jaxpr/kgnqj,njkd->nqkgd/dot_general | solution.py:87
  128.3 3.4 %convolution_convert_fusion.1 = bf16[256,2048]{1,0:T(8,128)(2,1)} fusion(bf16[256,512]{1,0:T(8,128)(2,1)S(1)} %reshape.444, bf16[2,512,2048]{2,1,0:T(8,128)(2,1)} %param.14), kind=kOutput, calls=%fused_computation.16 | convolution fusion | flops 537395200 | bytes 3407872 | tf_op jit(solution)/shard_map/dot_general | solution.py:119
  152.2 2.5 %copy.232 = bf16[512,2048]{1,0:T(8,128)(2,1)} copy(bf16[512,2048]{0,1:T(8,128)(2,1)S(1)} %get-tuple-element.42) | data formatting | bytes 4194304 | tf_op jit(solution)/shard_map/dot_general | solution.py:103
  156.1 9.7 %stack.619 = f32[2,4,1,64,320]{4,3,1,0,2:T(8,128)} concatenate(f32[2,4,1,1,320]{4,3,1,0,2:T(1,128)S(1)} %stack.684, f32[2,4,1,1,320]{4,3,1,0,2:T(1,128)S(1)} %stack.685, f32[2,4,1,1,320]{4,3,1,0,2:T(1,128)S(1)} %stack.686, f32[2,4,1,1,320]{4,3,1,0,2:T(1,128)S(1)} %stack.687, f32[2,4,1,1,320]{4,3,1,0,2:T(1,128)S(1)} %stack.688, f32[2,4,1,1,320]{4,3,1,0,2:T(1,128)S(1)} %stack.689, ...), dimensions={3} | concatenate | bytes 1310720 | tf_op jit(solution)/shard_map/stack | solution.py:38
  165.8 1.8 all-reduce.2.cloned.1.call-done
  167.6 1.9 fusion.8
  169.8 4.4 %collective-permute-start.1 = (bf16[256,2048]{1,0:T(8,128)(2,1)S(1)}, bf16[256,2048]{1,0:T(8,128)(2,1)}, u32[]{:S(2)}, u32[]{:S(2)}) collective-permute-start(bf16[256,2048]{1,0:T(8,128)(2,1)S(1)} %fusion.10), channel_id=1, source_target_pairs={{0,4},{4,8},{8,12},{12,16},{16,20},{20,24},{24,28},{1,5},{5,9},{9,... | collective-permute-start | bytes 3145736 | tf_op jit(solution)/shard_map/ppermute | solution.py:20
  178.7 16.3 %collective-permute-done.1 = bf16[256,2048]{1,0:T(8,128)(2,1)} collective-permute-done((bf16[256,2048]{1,0:T(8,128)(2,1)S(1)}, bf16[256,2048]{1,0:T(8,128)(2,1)}, u32[]{:S(2)}, u32[]{:S(2)}) %collective-permute-start.1) | collective-permute-done | bytes 1048608 | tf_op jit(solution)/shard_map/ppermute | solution.py:20
  198.5 1.7 multiply_reduce_fusion.3
  201.2 3.6 %fusion.146 = (f32[2,4,4,64]{3,1,2,0:T(4,128)S(1)}, f32[2,4,4,64,320]{4,3,1,2,0:T(8,128)}) fusion(f32[2,4,64,320]{3,2,1,0:T(8,128)S(1)} %bitcast.186, pred[4,320]{1,0:T(4,128)(4,1)} %add_compare_fusion, bf16[4,64,2,4,64]{1,0,4,3,2:T(4,128)(2,1)S(1)} %copy-done.4, bf16[1,320,2,64]{1,3,0,2:T(8,128)(2,1)S(1)} %bitcast.194, ...), kind=kOutput, calls=%fused_computation.203 | convolution fusion | flops 88473920 | bytes 3876096 | tf_op jit(solution)/shard_map/while/body/eval_jaxpr/sub | solution.py:85
  204.8 3.1 %fusion.37 = bf16[4,64,2,4,64]{1,4,3,2,0:T(8,128)(2,1)S(1)} fusion(bf16[1,320,2,64]{1,3,2,0:T(8,128)(2,1)S(1)} %bitcast.200, bf16[1,320,2,64]{1,3,2,0:T(8,128)(2,1)S(1)} %bitcast.201, bf16[1,320,2,64]{1,3,2,0:T(8,128)(2,1)S(1)} %bitcast.203, bf16[1,320,2,64]{1,3,2,0:T(8,128)(2,1)S(1)} %bitcast.206, f32[2,4,4,64,320]{4,3,1,2,0:T(8,128)} %get-tuple-element.234, ...), kind=kOutput, calls=%fused_computation.46 | convolution fusion | flops 86638592 | bytes 3219456 | tf_op jit(solution)/shard_map/while/body/eval_jaxpr/kgnqj,njkd->nqkgd/dot_general | solution.py:87
  208.5 3.3 %convolution_convert_fusion = bf16[256,2048]{1,0:T(8,128)(2,1)} fusion(bf16[256,512]{1,0:T(8,128)(2,1)S(1)} %reshape.447, bf16[2,512,2048]{2,1,0:T(8,128)(2,1)} %param.14), kind=kOutput, calls=%fused_computation.15 | convolution fusion | flops 537395200 | bytes 3407872 | tf_op jit(solution)/shard_map/dot_general | solution.py:119
  211.9 26.9 %reduce-scatter.2.cloned.1.call-done = bf16[256,512]{1,0:T(8,128)(2,1)} async-done(((bf16[256,2048]{1,0:T(8,128)(2,1)}), bf16[256,512]{1,0:T(8,128)(2,1)}) %reduce-scatter.2.cloned.1.call-update) | async-done | bytes 262160 | tf_op jit(solution)/shard_map/reduce_scatter | solution.py:124
  238.8 1.7 add_convert_fusion
  (297 shorter events, 112.6 us)
Async XLA Ops:
  6.5 161.0 %all-reduce.2.cloned.1.call-start = ((), (), s32[]{:S(2)}) async-start(), calls=%async_computation.1 | async-start | bytes 2097152 | tf_op jit(solution)/shard_map/psum | solution.py:121
  12.0 96.6 %collective-permute-start = (bf16[256,2048]{1,0:T(8,128)(2,1)}, bf16[256,2048]{1,0:T(8,128)(2,1)}, u32[]{:S(2)}, u32[]{:S(2)}) collective-permute-start(bf16[256,2048]{1,0:T(8,128)(2,1)} %fusion.13), channel_id=1, source_target_pairs={{0,4},{4,8},{8,12},{12,16},{16,20},{20,24},{24,28},{1,5},{5,9},{9,... | collective-permute-start | bytes 3145736 | tf_op jit(solution)/shard_map/ppermute | solution.py:20
  34.8 36.1 %copy-start.30 = (f32[8,320]{1,0:T(8,128)S(1)}, f32[8,320]{1,0:T(8,128)}, u32[]{:S(2)}) copy-start(f32[8,320]{1,0:T(8,128)} %get-tuple-element.122) | copy-start | bytes 30724
  34.8 36.8 %copy-start.28 = (f32[8,320]{1,0:T(8,128)S(1)}, f32[8,320]{1,0:T(8,128)}, u32[]{:S(2)}) copy-start(f32[8,320]{1,0:T(8,128)} %get-tuple-element.121) | copy-start | bytes 30724
  34.8 37.4 %copy-start.26 = (f32[8,320]{1,0:T(8,128)S(1)}, f32[8,320]{1,0:T(8,128)}, u32[]{:S(2)}) copy-start(f32[8,320]{1,0:T(8,128)} %get-tuple-element.120) | copy-start | bytes 30724
  34.8 38.0 %copy-start.24 = (f32[8,320]{1,0:T(8,128)S(1)}, f32[8,320]{1,0:T(8,128)}, u32[]{:S(2)}) copy-start(f32[8,320]{1,0:T(8,128)} %get-tuple-element.119) | copy-start | bytes 30724
  34.8 38.6 %copy-start.22 = (f32[8,320]{1,0:T(8,128)S(1)}, f32[8,320]{1,0:T(8,128)}, u32[]{:S(2)}) copy-start(f32[8,320]{1,0:T(8,128)} %get-tuple-element.118) | copy-start | bytes 30724
  34.8 39.2 %copy-start.21 = (f32[8,320]{1,0:T(8,128)S(1)}, f32[8,320]{1,0:T(8,128)}, u32[]{:S(2)}) copy-start(f32[8,320]{1,0:T(8,128)} %get-tuple-element.117) | copy-start | bytes 30724
  34.9 39.8 %copy-start.20 = (f32[8,320]{1,0:T(8,128)S(1)}, f32[8,320]{1,0:T(8,128)}, u32[]{:S(2)}) copy-start(f32[8,320]{1,0:T(8,128)} %get-tuple-element.116) | copy-start | bytes 30724
  34.9 40.4 %copy-start.19 = (f32[8,320]{1,0:T(8,128)S(1)}, f32[8,320]{1,0:T(8,128)}, u32[]{:S(2)}) copy-start(f32[8,320]{1,0:T(8,128)} %get-tuple-element.115) | copy-start | bytes 30724
  34.9 41.0 %copy-start.18 = (f32[8,320]{1,0:T(8,128)S(1)}, f32[8,320]{1,0:T(8,128)}, u32[]{:S(2)}) copy-start(f32[8,320]{1,0:T(8,128)} %get-tuple-element.114) | copy-start | bytes 30724
  34.9 41.6 %copy-start.17 = (f32[8,320]{1,0:T(8,128)S(1)}, f32[8,320]{1,0:T(8,128)}, u32[]{:S(2)}) copy-start(f32[8,320]{1,0:T(8,128)} %get-tuple-element.113) | copy-start | bytes 30724
  34.9 42.2 %copy-start.16 = (f32[8,320]{1,0:T(8,128)S(1)}, f32[8,320]{1,0:T(8,128)}, u32[]{:S(2)}) copy-start(f32[8,320]{1,0:T(8,128)} %get-tuple-element.112) | copy-start | bytes 30724
  34.9 42.8 %copy-start.15 = (f32[8,320]{1,0:T(8,128)S(1)}, f32[8,320]{1,0:T(8,128)}, u32[]{:S(2)}) copy-start(f32[8,320]{1,0:T(8,128)} %get-tuple-element.111) | copy-start | bytes 30724
  34.9 43.4 %copy-start.14 = (f32[8,320]{1,0:T(8,128)S(1)}, f32[8,320]{1,0:T(8,128)}, u32[]{:S(2)}) copy-start(f32[8,320]{1,0:T(8,128)} %get-tuple-element.110) | copy-start | bytes 30724
  34.9 44.0 %copy-start.13 = (f32[8,320]{1,0:T(8,128)S(1)}, f32[8,320]{1,0:T(8,128)}, u32[]{:S(2)}) copy-start(f32[8,320]{1,0:T(8,128)} %get-tuple-element.109) | copy-start | bytes 30724
  34.9 44.6 %copy-start.12 = (f32[8,320]{1,0:T(8,128)S(1)}, f32[8,320]{1,0:T(8,128)}, u32[]{:S(2)}) copy-start(f32[8,320]{1,0:T(8,128)} %get-tuple-element.108) | copy-start | bytes 30724
  34.9 45.2 %copy-start.11 = (f32[8,320]{1,0:T(8,128)S(1)}, f32[8,320]{1,0:T(8,128)}, u32[]{:S(2)}) copy-start(f32[8,320]{1,0:T(8,128)} %get-tuple-element.107) | copy-start | bytes 30724
  35.0 45.8 %copy-start.10 = (f32[8,320]{1,0:T(8,128)S(1)}, f32[8,320]{1,0:T(8,128)}, u32[]{:S(2)}) copy-start(f32[8,320]{1,0:T(8,128)} %get-tuple-element.106) | copy-start | bytes 30724
  35.0 46.4 %copy-start.9 = (f32[8,320]{1,0:T(8,128)S(1)}, f32[8,320]{1,0:T(8,128)}, u32[]{:S(2)}) copy-start(f32[8,320]{1,0:T(8,128)} %get-tuple-element.105) | copy-start | bytes 30724
  131.8 107.0 %reduce-scatter.2.cloned.1.call-start = ((), (), s32[]{:S(2)}) async-start(), calls=%async_computation.2 | async-start | bytes 1310720 | tf_op jit(solution)/shard_map/reduce_scatter | solution.py:124
  156.1 13.4 %copy-start.46 = (f32[1,2048]{1,0:T(1,128)S(1)}, f32[1,2048]{1,0:T(1,128)}, u32[]{:S(2)}) copy-start(f32[1,2048]{1,0:T(1,128)} %get-tuple-element.81) | copy-start | bytes 24580
  169.8 25.2 %collective-permute-start.1 = (bf16[256,2048]{1,0:T(8,128)(2,1)S(1)}, bf16[256,2048]{1,0:T(8,128)(2,1)}, u32[]{:S(2)}, u32[]{:S(2)}) collective-permute-start(bf16[256,2048]{1,0:T(8,128)(2,1)S(1)} %fusion.10), channel_id=1, source_target_pairs={{0,4},{4,8},{8,12},{12,16},{16,20},{20,24},{24,28},{1,5},{5,9},{9,... | collective-permute-start | bytes 3145736 | tf_op jit(solution)/shard_map/ppermute | solution.py:20
  176.1 18.9 %copy-start.52 = (bf16[2,2048,128]{2,1,0:T(8,128)(2,1)S(1)}, bf16[2,2048,128]{2,1,0:T(8,128)(2,1)}, u32[]{:S(2)}) copy-start(bf16[2,2048,128]{2,1,0:T(8,128)(2,1)} %param.13) | copy-start | bytes 3145732
  (34 other events, 167.8 us)
Sparse Core Ops, SparseCore 0:
  131.9 35.6 all-reduce.1
  212.0 26.7 reduce-scatter.1
where the time goes:
time: 251 us; the launch traced here: 247 us
  local copies, waits for them, and re-layouts  125 us (50%)
  waiting for transfers between devices  45 us (18%)
  matrix products  38.5 us (15%)
  between operations  14.4 us (6%)
  other arithmetic  14.2 us (6%)
  starting transfers between devices  10.5 us (4%)
    another operation x130, local copies, waits for them, and re-layouts, segment_bias(): return jnp.stack(rows, axis=1)  93.1 us
    reduce_scatter x1, waiting for transfers between devices, local(): lax.psum_scatter(partial_value.astype(jnp.bfloat16), 'tp', scatter_dimens...  26.9 us
    ppermute x2, waiting for transfers between devices, passed_along(): lax.ppermute(value, axis, [(source, source + steps) for source in range(i...  16.3 us
    dot_general x3, local copies, waits for them, and re-layouts, local(): jnp.dot(normed, w_query[layer_index], preferred_element_type=jnp.float32)  10.3 us
    ppermute x2, starting transfers between devices, passed_along(): lax.ppermute(value, axis, [(source, source + steps) for source in range(i...  10.3 us
    slice x8, local copies, waits for them, and re-layouts, one_block(): value_rows[q * SEG:q * SEG + span]  8.32 us
    sub x2, matrix products, one_block(): expon = jnp.exp(scores - peak)  7.66 us
    dot_general x2, matrix products, local(): jnp.dot(mixed, w_out[layer_index], preferred_element_type=jnp.float32)  6.73 us
  transfers between devices with their start and end apart: 4, of which 3 were waited for; matrix products, arithmetic and copies ran while one was open for 52% of the time, Pallas kernels for 0%

commit v1 on v0

v1 whole, which is shorter than its diff:
```python
import functools

import jax
import jax.numpy as jnp
from jax import lax
from jax.experimental import pallas as pl
from jax.experimental.pallas import tpu as pltpu
from jax.sharding import PartitionSpec as P

HEAD_DIM = 64
SEG = 64
LEFT = 4
CLIP = 128
LAYERS = 2
SPAN = (LEFT + 1) * SEG
LINE = 384

norm_eps = 1e-06
masked_score = -1e30
F32 = jnp.float32
BF16 = jnp.bfloat16


def seg_rows(seg):
    return pl.ds(pl.multiple_of(seg * SEG, SEG), SEG)


def send(src, dst, send_sem, recv_sem, device):
    return pltpu.make_async_remote_copy(
        src_ref=src,
        dst_ref=dst,
        send_sem=send_sem,
        recv_sem=recv_sem,
        device_id=device,
        device_id_type=pl.DeviceIdType.MESH,
    )


def row_norm(x, gain):
    squared = jnp.mean(x * x, axis=-1, keepdims=True)
    return (x * lax.rsqrt(squared + norm_eps) * gain).astype(BF16)


def head_norm(x, gain_row, scale):
    width = x.shape[1]
    block = min(width, 256)
    row_head = lax.broadcasted_iota(jnp.int32, (block, block), 0) >> 6
    col_head = lax.broadcasted_iota(jnp.int32, (block, block), 1) >> 6
    spread = jnp.where(row_head == col_head, 1.0 / HEAD_DIM, 0.0).astype(BF16)
    gain = jnp.concatenate([gain_row] * (block // HEAD_DIM), axis=1) * scale
    outs = []
    for lower in range(0, width, block):
        part = x[:, lower : lower + block]
        squares = part * part
        high = squares.astype(BF16)
        low = (squares - high.astype(F32)).astype(BF16)
        mean = jnp.dot(high, spread, preferred_element_type=F32) + jnp.dot(
            low, spread, preferred_element_type=F32
        )
        outs.append((part * lax.rsqrt(mean + norm_eps) * gain).astype(BF16))
    return outs[0] if len(outs) == 1 else jnp.concatenate(outs, axis=1)


def body(
    n_sp, n_tp,
    stream, attn_gain, w_query, w_key, w_value, w_out, query_gain, key_gain, rel_bias,
    out,
    cur0, cur1, normed, wq, wk, wv, wo, queries, pair_made, halo, kdup, vdup, bias, mixed,
    psend, precv, own0, xsend, xrecv,
    psend1, precv1, own1, xsend1, xrecv1,
    w_sem, ps_sem, pr_sem, xs_sem, xr_sem, cs_sem, cr_sem, hs_sem, hr_sem,
    ps1_sem, pr1_sem, xs1_sem, xr1_sem,
):
    row_count, width = cur0.shape
    segs = row_count // SEG
    half = segs // 2
    q_width = wq.shape[2]
    kv_width = wk.shape[2]
    heads = q_width // HEAD_DIM
    kv_heads = kv_width // HEAD_DIM
    group = heads // kv_heads
    n_x = n_tp // 2
    feat = width // n_tp
    me_sp = lax.axis_index("sp")
    me_tp = lax.axis_index("tp")
    core = lax.rem(me_tp, 2)
    chip = lax.div(me_tp, 2)
    partner = {"tp": chip * 2 + 1 - core}

    def chip_at(k):
        return lax.rem(chip + k, n_x)

    def peer(k):
        return {"tp": chip_at(k) * 2 + core}

    loads = []

    def load(src, dst):
        copy = pltpu.make_async_copy(src, dst, w_sem.at[len(loads)])
        copy.start()
        loads.append(copy)
        return copy

    stream_load = load(stream, cur0)
    weight_loads = []
    for l in range(LAYERS):
        weight_loads.append(
            [
                load(w_key.at[l], wk.at[l]),
                load(w_value.at[l], wv.at[l]),
                load(w_query.at[l], wq.at[l]),
                load(w_out.at[l], wo.at[l]),
            ]
        )

    barrier = pltpu.get_barrier_semaphore()
    pl.semaphore_signal(barrier, inc=1, device_id=partner, device_id_type=pl.DeviceIdType.MESH)
    for k in range(1, n_x):
        pl.semaphore_signal(barrier, inc=1, device_id=peer(k), device_id_type=pl.DeviceIdType.MESH)

    @pl.when(me_sp > 0)
    def _():
        pl.semaphore_signal(
            barrier, inc=1, device_id={"sp": me_sp - 1}, device_id_type=pl.DeviceIdType.MESH
        )

    @pl.when(me_sp < n_sp - 1)
    def _():
        pl.semaphore_signal(
            barrier, inc=1, device_id={"sp": me_sp + 1}, device_id_type=pl.DeviceIdType.MESH
        )

    offset = lax.broadcasted_iota(jnp.int32, (2 * CLIP, LINE), 1)
    distance = jnp.clip(LEFT * SEG + SEG - 1 - offset, -CLIP, CLIP) + CLIP
    onehot = (lax.broadcasted_iota(jnp.int32, (2 * CLIP, LINE), 0) == distance).astype(F32)
    far = (distance[:1] == 2 * CLIP).astype(F32)
    for l in range(LAYERS):
        table = rel_bias[l]
        line = jnp.dot(
            table[:, : 2 * CLIP], onehot, precision=lax.Precision.HIGHEST, preferred_element_type=F32
        ) + table[:, 2 * CLIP :] * far
        for h in range(heads):
            spread = jnp.broadcast_to(line[h : h + 1], (SEG, LINE))
            turned = pltpu.roll(spread, LINE - (SEG - 1), 1, stride=1, stride_axis=0)
            bias[l, h * SEG : (h + 1) * SEG, :] = turned

    for kv in range(kv_heads):
        vdup[kv, :, 128:] = jnp.ones((2 * row_count, 128), BF16)

    at_edge = jnp.logical_or(me_sp == 0, me_sp == n_sp - 1)

    @pl.when(at_edge)
    def _():
        pl.semaphore_wait(barrier, n_x + min(n_sp - 1, 1))

    @pl.when(jnp.logical_not(at_edge))
    def _():
        pl.semaphore_wait(barrier, n_x + 2)

    def keys_values(l, rows_in):
        both = jnp.concatenate([wk[l], wv[l]], axis=1)
        flat = jnp.dot(rows_in, both, preferred_element_type=F32)
        keys = head_norm(flat[:, :kv_width], key_gain[l : l + 1], 1.0)
        return keys, flat[:, kv_width:].astype(BF16)

    def make_queries(l, rows_in):
        flat = jnp.dot(rows_in, wq[l], preferred_element_type=F32)
        return head_norm(flat, query_gain[l : l + 1], HEAD_DIM ** (-0.5))

    def put_dup(keys, values, rows):
        for kv in range(kv_heads):
            cols = slice(kv * HEAD_DIM, (kv + 1) * HEAD_DIM)
            kdup[kv, rows, :] = jnp.concatenate([keys[:, cols]] * 2, axis=1)
            vdup[kv, rows, :128] = jnp.concatenate([values[:, cols]] * 2, axis=1)

    def halo_copy(l, seg):
        rows = seg_rows(seg)
        return send(
            pair_made.at[l, rows],
            halo.at[l, rows],
            hs_sem.at[l, seg],
            hr_sem.at[l, seg],
            {"sp": lax.rem(me_sp + 1, n_sp)},
        )

    def start_halo(l, which):
        @pl.when(me_sp < n_sp - 1)
        def _():
            for seg in which:
                halo_copy(l, seg).start()

    def finish_halo(l):
        @pl.when(me_sp > 0)
        def _():
            for seg in range(segs):
                halo_copy(l, seg).wait_recv()
            got = halo[l]
            put_dup(got[:, :kv_width], got[:, kv_width:], slice(0, row_count))

        @pl.when(me_sp == 0)
        def _():
            none = jnp.zeros((row_count, kv_width), BF16)
            put_dup(none, none, slice(0, row_count))

    def end_halo_sends(l):
        @pl.when(me_sp < n_sp - 1)
        def _():
            for seg in range(segs):
                halo_copy(l, seg).wait_send()

    lane = lax.broadcasted_iota(jnp.int32, (SEG, 128), 1)
    low_half = lane < HEAD_DIM

    def attend(l, seg):
        rows = seg_rows(seg)
        window = pl.ds(pl.multiple_of(seg * SEG, SEG), SPAN)
        key_pos = lax.broadcasted_iota(jnp.int32, (1, SPAN), 1)
        inside = me_sp * row_count + (seg - LEFT) * SEG + key_pos >= 0
        shut = jnp.where(inside, 0.0, masked_score)
        for kv in range(kv_heads):
            stack = []
            for p in range(group // 2):
                lower = (kv * group + 2 * p) * HEAD_DIM
                tile = queries[rows, lower : lower + 128]
                none = jnp.zeros_like(tile)
                stack += [jnp.where(low_half, tile, none), jnp.where(low_half, none, tile)]
            stacked = jnp.concatenate(stack, axis=0)
            scores = lax.dot_general(
                stacked, kdup[kv, window, :], (((1,), (1,)), ((), ())), preferred_element_type=F32
            )
            base = kv * group * SEG
            scores = scores + bias[l, base : base + group * SEG, :SPAN] + shut
            peak = jnp.max(scores, axis=-1, keepdims=True)
            expon = jnp.exp(scores - peak).astype(BF16)
            summed = jnp.dot(expon, vdup[kv, window, :], preferred_element_type=F32)
            made = summed[:, :128] / summed[:, 128:]
            for p in range(group // 2):
                lower = (kv * group + 2 * p) * HEAD_DIM
                even = made[2 * p * SEG : (2 * p + 1) * SEG]
                odd = made[(2 * p + 1) * SEG : (2 * p + 2) * SEG]
                mixed[:, lower : lower + 128] = jnp.where(low_half, even, odd).astype(BF16)

    def project_out(l, lower, size):
        cols = pl.ds(pl.multiple_of(lower, 128), size)
        return jnp.dot(mixed[...], wo[l, :, cols], preferred_element_type=F32)

    stream_load.wait()
    normed[...] = row_norm(cur0[...].astype(F32), attn_gain[0:1])
    weight_loads[0][0].wait()
    weight_loads[0][1].wait()
    keys, values = keys_values(0, normed[...])
    pair_made[0] = jnp.concatenate([keys, values], axis=1)
    start_halo(0, range(segs))
    put_dup(keys, values, slice(row_count, 2 * row_count))
    weight_loads[0][2].wait()
    queries[...] = make_queries(0, normed[...])
    weight_loads[0][3].wait()
    finish_halo(0)

    def partner_copy(i):
        return send(psend.at[i], precv.at[i], ps_sem.at[i], pr_sem.at[i], partner)

    def chip_copy(i, k):
        return send(
            xsend.at[i], xrecv.at[k - 1, i], xs_sem.at[k - 1, i], xr_sem.at[k - 1, i], peer(k)
        )

    def rows_copy(i):
        rows = seg_rows(core * half + i)
        return send(cur1.at[rows], cur1.at[rows], cs_sem.at[i], cr_sem.at[i], partner)

    out_step = min(width, 512)

    def first_out(i, carry):
        attend(0, (1 - core) * half + i)
        for lower in range(0, width, out_step):
            psend[i, :, lower : lower + out_step] = project_out(0, lower, out_step).astype(BF16)
        partner_copy(i).start()
        attend(0, core * half + i)
        for lower in range(0, width, out_step):
            own0[i, :, lower : lower + out_step] = project_out(0, lower, out_step)
        partner_copy(i).wait_recv()
        both = own0[i] + precv[i].astype(F32)
        own0[i] = both
        xsend[i] = both.astype(BF16)
        for k in range(1, n_x):
            chip_copy(i, k).start()
        return carry

    lax.fori_loop(0, half, first_out, 0)

    for l in range(1, LAYERS):
        for copy in weight_loads[l]:
            copy.wait()

    for i in range(half):
        mine = core * half + i
        theirs = (1 - core) * half + i
        total = own0[i]
        for k in range(1, n_x):
            chip_copy(i, k).wait_recv()
            total = total + xrecv[k - 1, i].astype(F32)
        cur1[seg_rows(mine), :] = (cur0[seg_rows(mine), :].astype(F32) + total).astype(BF16)
        rows_copy(i).start()
        normed[0:SEG, :] = row_norm(cur1[seg_rows(mine), :].astype(F32), attn_gain[1:2])
        send(
            cur1.at[seg_rows(theirs)], cur1.at[seg_rows(theirs)], cs_sem.at[i], cr_sem.at[i], partner
        ).wait_recv()
        normed[SEG : 2 * SEG, :] = row_norm(cur1[seg_rows(theirs), :].astype(F32), attn_gain[1:2])
        rows_in = normed[0 : 2 * SEG, :]
        keys, values = keys_values(1, rows_in)
        made = jnp.concatenate([keys, values], axis=1)
        for n, seg in enumerate((mine, theirs)):
            part = slice(n * SEG, (n + 1) * SEG)
            pair_made[1, seg_rows(seg), :] = made[part]
        start_halo(1, (mine, theirs))
        for n, seg in enumerate((mine, theirs)):
            part = slice(n * SEG, (n + 1) * SEG)
            put_dup(keys[part], values[part], seg_rows(seg + segs))
        made_q = make_queries(1, rows_in)
        for n, seg in enumerate((mine, theirs)):
            queries[seg_rows(seg), :] = made_q[n * SEG : (n + 1) * SEG]
    finish_halo(1)

    def partner_copy1(s):
        return send(psend1.at[s], precv1.at[s], ps1_sem.at[s], pr1_sem.at[s], partner)

    def chip_copy1(s, k):
        return send(
            xsend1.at[k - 1, s],
            xrecv1.at[k - 1, s],
            xs1_sem.at[k - 1, s],
            xr1_sem.at[k - 1, s],
            peer(k),
        )

    def last_sends(s):
        partner_copy1(s).wait_recv()
        for k in range(n_x):
            both = own1[s, k] + precv1[s, k].astype(F32)
            if k == 0:
                own1[s, k] = both
            else:
                xsend1[k - 1, s] = both.astype(BF16)
                chip_copy1(s, k).start()

    def last_out(s, carry):
        attend(1, s)
        for k in range(n_x):
            lower = (chip_at(k) * 2 + 1 - core) * feat
            psend1[s, k] = project_out(1, lower, feat).astype(BF16)
        partner_copy1(s).start()
        for k in range(n_x):
            lower = (chip_at(k) * 2 + core) * feat
            own1[s, k] = project_out(1, lower, feat)

        @pl.when(s > 0)
        def _():
            last_sends(s - 1)

        return carry

    lax.fori_loop(0, segs, last_out, 0)
    last_sends(segs - 1)
    my_cols = pl.ds(pl.multiple_of(me_tp * feat, 128), feat)
    for s in range(segs):
        rows = slice(s * SEG, (s + 1) * SEG)
        total = own1[s, 0]
        for k in range(1, n_x):
            chip_copy1(s, k).wait_recv()
            total = total + xrecv1[k - 1, s].astype(F32)
        out[rows, :] = (cur1[rows, my_cols].astype(F32) + total).astype(BF16)

    for i in range(half):
        partner_copy(i).wait_send()
        rows_copy(i).wait_send()
        for k in range(1, n_x):
            chip_copy(i, k).wait_send()
    for s in range(segs):
        partner_copy1(s).wait_send()
        for k in range(1, n_x):
            chip_copy1(s, k).wait_send()
    for l in range(LAYERS):
        end_halo_sends(l)


def local(n_sp, n_tp, stream, attn_gain, w_query, w_key, w_value, w_out, query_gain, key_gain, rel_bias):
    row_count, width = stream.shape
    segs = row_count // SEG
    assert row_count == LEFT * SEG and n_tp % 2 == 0
    half = segs // 2
    n_x = n_tp // 2
    feat = width // n_tp
    q_width = w_query.shape[2]
    kv_width = w_key.shape[2]
    kv_heads = kv_width // HEAD_DIM
    heads = q_width // HEAD_DIM
    others = max(n_x - 1, 1)
    dma = pltpu.SemaphoreType.DMA
    anyw = pl.BlockSpec(memory_space=pl.ANY)
    vmem = pl.BlockSpec(memory_space=pltpu.VMEM)
    scratch = [
        pltpu.VMEM((row_count, width), BF16),
        pltpu.VMEM((row_count, width), BF16),
        pltpu.VMEM((row_count, width), BF16),
        pltpu.VMEM(w_query.shape, BF16),
        pltpu.VMEM(w_key.shape, BF16),
        pltpu.VMEM(w_value.shape, BF16),
        pltpu.VMEM(w_out.shape, BF16),
        pltpu.VMEM((row_count, q_width), BF16),
        pltpu.VMEM((LAYERS, row_count, 2 * kv_width), BF16),
        pltpu.VMEM((LAYERS, row_count, 2 * kv_width), BF16),
        pltpu.VMEM((kv_heads, 2 * row_count, 128), BF16),
        pltpu.VMEM((kv_heads, 2 * row_count, 256), BF16),
        pltpu.VMEM((LAYERS, heads * SEG, LINE), F32),
        pltpu.VMEM((SEG, q_width), BF16),
        pltpu.VMEM((half, SEG, width), BF16),
        pltpu.VMEM((half, SEG, width), BF16),
        pltpu.VMEM((half, SEG, width), F32),
        pltpu.VMEM((half, SEG, width), BF16),
        pltpu.VMEM((others, half, SEG, width), BF16),
        pltpu.VMEM((segs, n_x, SEG, feat), BF16),
        pltpu.VMEM((segs, n_x, SEG, feat), BF16),
        pltpu.VMEM((segs, n_x, SEG, feat), F32),
        pltpu.VMEM((others, segs, SEG, feat), BF16),
        pltpu.VMEM((others, segs, SEG, feat), BF16),
        dma((1 + 4 * LAYERS,)),
        dma((half,)), dma((half,)),
        dma((others, half)), dma((others, half)),
        dma((half,)), dma((half,)),
        dma((LAYERS, segs)), dma((LAYERS, segs)),
        dma((segs,)), dma((segs,)),
        dma((others, segs)), dma((others, segs)),
    ]
    return pl.pallas_call(
        functools.partial(body, n_sp, n_tp),
        out_shape=jax.ShapeDtypeStruct((row_count, feat), BF16),
        in_specs=[anyw, vmem, anyw, anyw, anyw, anyw, vmem, vmem, vmem],
        out_specs=vmem,
        scratch_shapes=scratch,
        compiler_params=pltpu.CompilerParams(
            collective_id=0, has_side_effects=True, vmem_limit_bytes=60 * 1024 * 1024
        ),
    )(stream, attn_gain, w_query, w_key, w_value, w_out, query_gain, key_gain, rel_bias)


def solution(mesh):
    return jax.shard_map(
        functools.partial(local, mesh.shape["sp"], mesh.shape["tp"]),
        mesh=mesh,
        in_specs=(
            P("sp", None),
            P(),
            P(None, None, "tp"),
            P(None, None, "tp"),
            P(None, None, "tp"),
            P(None, "tp", None),
            P(),
            P(),
            P(None, "tp", None),
        ),
        out_specs=P("sp", "tp"),
        check_vma=False,
    )
```

time: 251 us -> 42.5 us (0.17)
  the two profiles are of different devices: /device:TPU:0 before, /device:TPU:27 now
where the time goes in v1:
time: 42.5 us; the launch traced here: 42.2 us
  Pallas kernels  40.5 us (95%)
  local copies, waits for them, and re-layouts  1.67 us (4%)
    pallas_call x1, Pallas kernels, local(): pl.pallas_call(functools.partial(body, n_sp, n_tp), out_shape=jax.ShapeDt...  40.5 us
    unnamed x1, local copies, waits for them, and re-layouts  1.67 us

profile of v1, /device:TPU:27, one launch (start us, length us, event | category | flops | bytes accessed | tf_op | source)
XLA Modules:
  0.0 42.2 jit_solution(16067919007113372494)
XLA Ops:
  0.0 40.5 %shard_map.91 = bf16[256,512]{1,0:T(8,128)(2,1)} custom-call(bf16[256,2048]{1,0:T(8,128)(2,1)} %stream.1, f32[2,2048]{1,0:T(2,128)} %attn_gain.1, bf16[2,2048,512]{2,1,0:T(8,128)(2,1)} %w_query.1, bf16[2,2048,128]{2,1,0:T(8,128)(2,1)} %w_key.1, bf16[2,2048,128]{2,1,0:T(8,128)(2,1)} %w_value.1, bf16[2,512,2048]{2,1,0:T(8,128)(2,1)} %w_out.1, ...), custom_call_target="tpu_custom_call" | custom-call | tf_op jit(solution)/shard_map/pallas_call | solution.py:435
  40.5 1.7 %copy.11 = bf16[256,512]{1,0:T(8,128)(2,1)} copy(bf16[256,512]{1,0:T(8,128)(2,1)} %shard_map.91) | data formatting | bytes 524288

commit v2 on v1

--- a/solution.py
+++ b/solution.py
@@ -63,8 +63,9 @@
 
 def body(
     n_sp, n_tp,
-    stream, attn_gain, w_query, w_key, w_value, w_out, query_gain, key_gain, rel_bias,
+    stream, attn_gain_in, w_query, w_key, w_value, w_out, query_gain_in, key_gain_in, rel_bias_in,
     out,
+    attn_gain, query_gain, key_gain, rel_bias,
     cur0, cur1, normed, wq, wk, wv, wo, queries, pair_made, halo, kdup, vdup, bias, mixed,
     psend, precv, own0, xsend, xrecv,
     psend1, precv1, own1, xsend1, xrecv1,
@@ -93,6 +94,23 @@
     def peer(k):
         return {"tp": chip_at(k) * 2 + core}
 
+    barrier = pltpu.get_barrier_semaphore()
+    pl.semaphore_signal(barrier, inc=1, device_id=partner, device_id_type=pl.DeviceIdType.MESH)
+    for k in range(1, n_x):
+        pl.semaphore_signal(barrier, inc=1, device_id=peer(k), device_id_type=pl.DeviceIdType.MESH)
+
+    @pl.when(me_sp > 0)
+    def _():
+        pl.semaphore_signal(
+            barrier, inc=1, device_id={"sp": me_sp - 1}, device_id_type=pl.DeviceIdType.MESH
+        )
+
+    @pl.when(me_sp < n_sp - 1)
+    def _():
+        pl.semaphore_signal(
+            barrier, inc=1, device_id={"sp": me_sp + 1}, device_id_type=pl.DeviceIdType.MESH
+        )
+
     loads = []
 
     def load(src, dst):
@@ -102,6 +120,12 @@
         return copy
 
     stream_load = load(stream, cur0)
+    gain_loads = [
+        load(attn_gain_in, attn_gain),
+        load(query_gain_in, query_gain),
+        load(key_gain_in, key_gain),
+        load(rel_bias_in, rel_bias),
+    ]
     weight_loads = []
     for l in range(LAYERS):
         weight_loads.append(
@@ -113,28 +137,11 @@
             ]
         )
 
-    barrier = pltpu.get_barrier_semaphore()
-    pl.semaphore_signal(barrier, inc=1, device_id=partner, device_id_type=pl.DeviceIdType.MESH)
-    for k in range(1, n_x):
-        pl.semaphore_signal(barrier, inc=1, device_id=peer(k), device_id_type=pl.DeviceIdType.MESH)
-
-    @pl.when(me_sp > 0)
-    def _():
-        pl.semaphore_signal(
-            barrier, inc=1, device_id={"sp": me_sp - 1}, device_id_type=pl.DeviceIdType.MESH
-        )
-
-    @pl.when(me_sp < n_sp - 1)
-    def _():
-        pl.semaphore_signal(
-            barrier, inc=1, device_id={"sp": me_sp + 1}, device_id_type=pl.DeviceIdType.MESH
-        )
-
-    offset = lax.broadcasted_iota(jnp.int32, (2 * CLIP, LINE), 1)
-    distance = jnp.clip(LEFT * SEG + SEG - 1 - offset, -CLIP, CLIP) + CLIP
-    onehot = (lax.broadcasted_iota(jnp.int32, (2 * CLIP, LINE), 0) == distance).astype(F32)
-    far = (distance[:1] == 2 * CLIP).astype(F32)
-    for l in range(LAYERS):
+    def build_bias(l):
+        offset = lax.broadcasted_iota(jnp.int32, (2 * CLIP, LINE), 1)
+        distance = jnp.clip(LEFT * SEG + SEG - 1 - offset, -CLIP, CLIP) + CLIP
+        onehot = (lax.broadcasted_iota(jnp.int32, (2 * CLIP, LINE), 0) == distance).astype(F32)
+        far = (distance[:1] == 2 * CLIP).astype(F32)
         table = rel_bias[l]
         line = jnp.dot(
             table[:, : 2 * CLIP], onehot, precision=lax.Precision.HIGHEST, preferred_element_type=F32
@@ -147,16 +154,6 @@
     for kv in range(kv_heads):
         vdup[kv, :, 128:] = jnp.ones((2 * row_count, 128), BF16)
 
-    at_edge = jnp.logical_or(me_sp == 0, me_sp == n_sp - 1)
-
-    @pl.when(at_edge)
-    def _():
-        pl.semaphore_wait(barrier, n_x + min(n_sp - 1, 1))
-
-    @pl.when(jnp.logical_not(at_edge))
-    def _():
-        pl.semaphore_wait(barrier, n_x + 2)
-
     def keys_values(l, rows_in):
         both = jnp.concatenate([wk[l], wv[l]], axis=1)
         flat = jnp.dot(rows_in, both, preferred_element_type=F32)
@@ -189,18 +186,17 @@
             for seg in which:
                 halo_copy(l, seg).start()
 
-    def finish_halo(l):
+    def finish_halo(l, seg):
         @pl.when(me_sp > 0)
         def _():
-            for seg in range(segs):
-                halo_copy(l, seg).wait_recv()
-            got = halo[l]
-            put_dup(got[:, :kv_width], got[:, kv_width:], slice(0, row_count))
+            halo_copy(l, seg).wait_recv()
+            got = halo[l, seg_rows(seg), :]
+            put_dup(got[:, :kv_width], got[:, kv_width:], seg_rows(seg))
 
         @pl.when(me_sp == 0)
         def _():
-            none = jnp.zeros((row_count, kv_width), BF16)
-            put_dup(none, none, slice(0, row_count))
+            none = jnp.zeros((SEG, kv_width), BF16)
+            put_dup(none, none, seg_rows(seg))
 
     def end_halo_sends(l):
         @pl.when(me_sp < n_sp - 1)
@@ -245,17 +241,36 @@
         return jnp.dot(mixed[...], wo[l, :, cols], preferred_element_type=F32)
 
     stream_load.wait()
+    for copy in gain_loads:
+        copy.wait()
     normed[...] = row_norm(cur0[...].astype(F32), attn_gain[0:1])
     weight_loads[0][0].wait()
     weight_loads[0][1].wait()
     keys, values = keys_values(0, normed[...])
     pair_made[0] = jnp.concatenate([keys, values], axis=1)
-    start_halo(0, range(segs))
+    at_edge = jnp.logical_or(me_sp == 0, me_sp == n_sp - 1)
+
+    @pl.when(at_edge)
+    def _():
+        pl.semaphore_wait(barrier, n_x + min(n_sp - 1, 1))
+
+    @pl.when(jnp.logical_not(at_edge))
+    def _():
+        pl.semaphore_wait(barrier, n_x + 2)
+
+    start_halo(0, reversed(range(segs)))
     put_dup(keys, values, slice(row_count, 2 * row_count))
     weight_loads[0][2].wait()
     queries[...] = make_queries(0, normed[...])
+    build_bias(0)
+    build_bias(1)
     weight_loads[0][3].wait()
-    finish_halo(0)
+
+    def mine_at(i):
+        return (half - 1 - i) * 2 + core
+
+    def theirs_at(i):
+        return (half - 1 - i) * 2 + 1 - core
 
     def partner_copy(i):
         return send(psend.at[i], precv.at[i], ps_sem.at[i], pr_sem.at[i], partner)
@@ -266,17 +281,19 @@
         )
 
     def rows_copy(i):
-        rows = seg_rows(core * half + i)
+        rows = seg_rows(mine_at(i))
         return send(cur1.at[rows], cur1.at[rows], cs_sem.at[i], cr_sem.at[i], partner)
 
     out_step = min(width, 512)
 
     def first_out(i, carry):
-        attend(0, (1 - core) * half + i)
+        finish_halo(0, (half - 1 - i) * 2 + 1)
+        finish_halo(0, (half - 1 - i) * 2)
+        attend(0, theirs_at(i))
         for lower in range(0, width, out_step):
             psend[i, :, lower : lower + out_step] = project_out(0, lower, out_step).astype(BF16)
         partner_copy(i).start()
-        attend(0, core * half + i)
+        attend(0, mine_at(i))
         for lower in range(0, width, out_step):
             own0[i, :, lower : lower + out_step] = project_out(0, lower, out_step)
         partner_copy(i).wait_recv()
@@ -294,8 +311,8 @@
             copy.wait()
 
     for i in range(half):
-        mine = core * half + i
-        theirs = (1 - core) * half + i
+        mine = mine_at(i)
+        theirs = theirs_at(i)
         total = own0[i]
         for k in range(1, n_x):
             chip_copy(i, k).wait_recv()
@@ -320,7 +337,6 @@
         made_q = make_queries(1, rows_in)
         for n, seg in enumerate((mine, theirs)):
             queries[seg_rows(seg), :] = made_q[n * SEG : (n + 1) * SEG]
-    finish_halo(1)
 
     def partner_copy1(s):
         return send(psend1.at[s], precv1.at[s], ps1_sem.at[s], pr1_sem.at[s], partner)
@@ -345,7 +361,8 @@
                 chip_copy1(s, k).start()
 
     def last_out(s, carry):
-        attend(1, s)
+        finish_halo(1, segs - 1 - s)
+        attend(1, segs - 1 - s)
         for k in range(n_x):
             lower = (chip_at(k) * 2 + 1 - core) * feat
             psend1[s, k] = project_out(1, lower, feat).astype(BF16)
@@ -364,7 +381,7 @@
     last_sends(segs - 1)
     my_cols = pl.ds(pl.multiple_of(me_tp * feat, 128), feat)
     for s in range(segs):
-        rows = slice(s * SEG, (s + 1) * SEG)
+        rows = slice((segs - 1 - s) * SEG, (segs - s) * SEG)
         total = own1[s, 0]
         for k in range(1, n_x):
             chip_copy1(s, k).wait_recv()
@@ -400,6 +417,10 @@
     anyw = pl.BlockSpec(memory_space=pl.ANY)
     vmem = pl.BlockSpec(memory_space=pltpu.VMEM)
     scratch = [
+        pltpu.VMEM(attn_gain.shape, F32),
+        pltpu.VMEM(query_gain.shape, F32),
+        pltpu.VMEM(key_gain.shape, F32),
+        pltpu.VMEM(rel_bias.shape, F32),
         pltpu.VMEM((row_count, width), BF16),
         pltpu.VMEM((row_count, width), BF16),
         pltpu.VMEM((row_count, width), BF16),
@@ -424,7 +445,7 @@
         pltpu.VMEM((segs, n_x, SEG, feat), F32),
         pltpu.VMEM((others, segs, SEG, feat), BF16),
         pltpu.VMEM((others, segs, SEG, feat), BF16),
-        dma((1 + 4 * LAYERS,)),
+        dma((5 + 4 * LAYERS,)),
         dma((half,)), dma((half,)),
         dma((others, half)), dma((others, half)),
         dma((half,)), dma((half,)),
@@ -435,7 +456,7 @@
     return pl.pallas_call(
         functools.partial(body, n_sp, n_tp),
         out_shape=jax.ShapeDtypeStruct((row_count, feat), BF16),
-        in_specs=[anyw, vmem, anyw, anyw, anyw, anyw, vmem, vmem, vmem],
+        in_specs=[anyw] * 9,
         out_specs=vmem,
         scratch_shapes=scratch,
         compiler_params=pltpu.CompilerParams(

time: 42.5 us -> 39.1 us (0.920)
  Pallas kernels: 40.5 us -> 37.3 us
    pallas_call x1, Pallas kernels: 40.5 us -> 37.3 us  [local(): pl.pallas_call(functools.partial(body, n_sp, n_tp), out_shape=jax.ShapeDt...]
where the time goes in v2:
time: 39.1 us; the launch traced here: 39 us
  Pallas kernels  37.3 us (95%)
  local copies, waits for them, and re-layouts  1.67 us (4%)
    pallas_call x1, Pallas kernels, local(): pl.pallas_call(functools.partial(body, n_sp, n_tp), out_shape=jax.ShapeDt...  37.3 us
    unnamed x1, local copies, waits for them, and re-layouts  1.67 us

profile of v2, /device:TPU:27, one launch (start us, length us, event | category | flops | bytes accessed | tf_op | source)
XLA Modules:
  0.0 39.0 jit_solution(2389156471648888609)
XLA Ops:
  0.0 37.3 %shard_map.91 = bf16[256,512]{1,0:T(8,128)(2,1)} custom-call(bf16[256,2048]{1,0:T(8,128)(2,1)} %stream.1, f32[2,2048]{1,0:T(2,128)} %attn_gain_in.1, bf16[2,2048,512]{2,1,0:T(8,128)(2,1)} %w_query.1, bf16[2,2048,128]{2,1,0:T(8,128)(2,1)} %w_key.1, bf16[2,2048,128]{2,1,0:T(8,128)(2,1)} %w_value.1, bf16[2,512,2048]{2,1,0:T(8,128)(2,1)} %w_out.1, ...), custom_call_target="tpu_custom_call" | custom-call | tf_op jit(solution)/shard_map/pallas_call | solution.py:456
  37.3 1.7 %copy.11 = bf16[256,512]{1,0:T(8,128)(2,1)} copy(bf16[256,512]{1,0:T(8,128)(2,1)} %shard_map.91) | data formatting | bytes 524288

commit v3 on v2

--- a/solution.py
+++ b/solution.py
@@ -14,6 +14,7 @@
 LAYERS = 2
 SPAN = (LEFT + 1) * SEG
 LINE = 384
+SUBS = 2
 
 norm_eps = 1e-06
 masked_score = -1e30
@@ -119,7 +120,9 @@
         loads.append(copy)
         return copy
 
-    stream_load = load(stream, cur0)
+    part_rows = row_count // 2
+    parts = [pl.ds(n * part_rows, part_rows) for n in (1, 0)]
+    stream_loads = [load(stream.at[part], cur0.at[part]) for part in parts]
     gain_loads = [
         load(attn_gain_in, attn_gain),
         load(query_gain_in, query_gain),
@@ -240,26 +243,34 @@
         cols = pl.ds(pl.multiple_of(lower, 128), size)
         return jnp.dot(mixed[...], wo[l, :, cols], preferred_element_type=F32)
 
-    stream_load.wait()
-    for copy in gain_loads:
-        copy.wait()
-    normed[...] = row_norm(cur0[...].astype(F32), attn_gain[0:1])
-    weight_loads[0][0].wait()
-    weight_loads[0][1].wait()
-    keys, values = keys_values(0, normed[...])
-    pair_made[0] = jnp.concatenate([keys, values], axis=1)
-    at_edge = jnp.logical_or(me_sp == 0, me_sp == n_sp - 1)
-
-    @pl.when(at_edge)
-    def _():
-        pl.semaphore_wait(barrier, n_x + min(n_sp - 1, 1))
-
-    @pl.when(jnp.logical_not(at_edge))
-    def _():
-        pl.semaphore_wait(barrier, n_x + 2)
-
-    start_halo(0, reversed(range(segs)))
-    put_dup(keys, values, slice(row_count, 2 * row_count))
+    def meet():
+        at_edge = jnp.logical_or(me_sp == 0, me_sp == n_sp - 1)
+
+        @pl.when(at_edge)
+        def _():
+            pl.semaphore_wait(barrier, n_x + min(n_sp - 1, 1))
+
+        @pl.when(jnp.logical_not(at_edge))
+        def _():
+            pl.semaphore_wait(barrier, n_x + 2)
+
+    for n, part in enumerate(parts):
+        stream_loads[n].wait()
+        if n == 0:
+            gain_loads[0].wait()
+        normed[part, :] = row_norm(cur0[part, :].astype(F32), attn_gain[0:1])
+        if n == 0:
+            for copy in gain_loads[1:]:
+                copy.wait()
+            weight_loads[0][0].wait()
+            weight_loads[0][1].wait()
+        keys, values = keys_values(0, normed[part, :])
+        pair_made[0, part, :] = jnp.concatenate([keys, values], axis=1)
+        if n == 0:
+            meet()
+        first_seg = (1 - n) * (segs // 2)
+        start_halo(0, reversed(range(first_seg, first_seg + segs // 2)))
+        put_dup(keys, values, pl.ds(row_count + (1 - n) * part_rows, part_rows))
     weight_loads[0][2].wait()
     queries[...] = make_queries(0, normed[...])
     build_bias(0)
@@ -275,14 +286,24 @@
     def partner_copy(i):
         return send(psend.at[i], precv.at[i], ps_sem.at[i], pr_sem.at[i], partner)
 
-    def chip_copy(i, k):
+    sub = SEG // SUBS
+
+    def chip_copy(i, j, k):
+        rows = pl.ds(j * sub, sub)
         return send(
-            xsend.at[i], xrecv.at[k - 1, i], xs_sem.at[k - 1, i], xr_sem.at[k - 1, i], peer(k)
-        )
-
-    def rows_copy(i):
-        rows = seg_rows(mine_at(i))
-        return send(cur1.at[rows], cur1.at[rows], cs_sem.at[i], cr_sem.at[i], partner)
+            xsend.at[i, rows],
+            xrecv.at[k - 1, i, rows],
+            xs_sem.at[k - 1, i, j],
+            xr_sem.at[k - 1, i, j],
+            peer(k),
+        )
+
+    def sub_rows(seg, j):
+        return pl.ds(pl.multiple_of(seg * SEG + j * sub, sub), sub)
+
+    def rows_copy(i, j, seg):
+        rows = sub_rows(seg, j)
+        return send(cur1.at[rows], cur1.at[rows], cs_sem.at[i, j], cr_sem.at[i, j], partner)
 
     out_step = min(width, 512)
 
@@ -297,11 +318,13 @@
         for lower in range(0, width, out_step):
             own0[i, :, lower : lower + out_step] = project_out(0, lower, out_step)
         partner_copy(i).wait_recv()
-        both = own0[i] + precv[i].astype(F32)
-        own0[i] = both
-        xsend[i] = both.astype(BF16)
-        for k in range(1, n_x):
-            chip_copy(i, k).start()
+        for j in range(SUBS):
+            rows = slice(j * sub, (j + 1) * sub)
+            both = own0[i, rows, :] + precv[i, rows, :].astype(F32)
+            own0[i, rows, :] = both
+            xsend[i, rows, :] = both.astype(BF16)
+            for k in range(1, n_x):
+                chip_copy(i, j, k).start()
         return carry
 
     lax.fori_loop(0, half, first_out, 0)
@@ -313,17 +336,21 @@
     for i in range(half):
         mine = mine_at(i)
         theirs = theirs_at(i)
-        total = own0[i]
-        for k in range(1, n_x):
-            chip_copy(i, k).wait_recv()
-            total = total + xrecv[k - 1, i].astype(F32)
-        cur1[seg_rows(mine), :] = (cur0[seg_rows(mine), :].astype(F32) + total).astype(BF16)
-        rows_copy(i).start()
-        normed[0:SEG, :] = row_norm(cur1[seg_rows(mine), :].astype(F32), attn_gain[1:2])
-        send(
-            cur1.at[seg_rows(theirs)], cur1.at[seg_rows(theirs)], cs_sem.at[i], cr_sem.at[i], partner
-        ).wait_recv()
-        normed[SEG : 2 * SEG, :] = row_norm(cur1[seg_rows(theirs), :].astype(F32), attn_gain[1:2])
+        for j in range(SUBS):
+            total = own0[i, j * sub : (j + 1) * sub, :]
+            for k in range(1, n_x):
+                chip_copy(i, j, k).wait_recv()
+                total = total + xrecv[k - 1, i, j * sub : (j + 1) * sub, :].astype(F32)
+            rows = sub_rows(mine, j)
+            summed = (cur0[rows, :].astype(F32) + total).astype(BF16)
+            cur1[rows, :] = summed
+            rows_copy(i, j, mine).start()
+            normed[j * sub : (j + 1) * sub, :] = row_norm(summed.astype(F32), attn_gain[1:2])
+        for j in range(SUBS):
+            rows_copy(i, j, theirs).wait_recv()
+            normed[SEG + j * sub : SEG + (j + 1) * sub, :] = row_norm(
+                cur1[sub_rows(theirs, j), :].astype(F32), attn_gain[1:2]
+            )
         rows_in = normed[0 : 2 * SEG, :]
         keys, values = keys_values(1, rows_in)
         made = jnp.concatenate([keys, values], axis=1)
@@ -390,9 +417,10 @@
 
     for i in range(half):
         partner_copy(i).wait_send()
-        rows_copy(i).wait_send()
-        for k in range(1, n_x):
-            chip_copy(i, k).wait_send()
+        for j in range(SUBS):
+            rows_copy(i, j, mine_at(i)).wait_send()
+            for k in range(1, n_x):
+                chip_copy(i, j, k).wait_send()
     for s in range(segs):
         partner_copy1(s).wait_send()
         for k in range(1, n_x):
@@ -414,7 +442,7 @@
     heads = q_width // HEAD_DIM
     others = max(n_x - 1, 1)
     dma = pltpu.SemaphoreType.DMA
-    anyw = pl.BlockSpec(memory_space=pl.ANY)
+    anyw = pl.BlockSpec(memory_space=pltpu.HBM)
     vmem = pl.BlockSpec(memory_space=pltpu.VMEM)
     scratch = [
         pltpu.VMEM(attn_gain.shape, F32),
@@ -445,17 +473,17 @@
         pltpu.VMEM((segs, n_x, SEG, feat), F32),
         pltpu.VMEM((others, segs, SEG, feat), BF16),
         pltpu.VMEM((others, segs, SEG, feat), BF16),
-        dma((5 + 4 * LAYERS,)),
+        dma((6 + 4 * LAYERS,)),
         dma((half,)), dma((half,)),
-        dma((others, half)), dma((others, half)),
-        dma((half,)), dma((half,)),
+        dma((others, half, SUBS)), dma((others, half, SUBS)),
+        dma((half, SUBS)), dma((half, SUBS)),
         dma((LAYERS, segs)), dma((LAYERS, segs)),
         dma((segs,)), dma((segs,)),
         dma((others, segs)), dma((others, segs)),
     ]
     return pl.pallas_call(
         functools.partial(body, n_sp, n_tp),
-        out_shape=jax.ShapeDtypeStruct((row_count, feat), BF16),
+        out_shape=pltpu.VMEM((row_count, feat), BF16),
         in_specs=[anyw] * 9,
         out_specs=vmem,
         scratch_shapes=scratch,

time: 39.1 us -> 37 us (0.946)
  Pallas kernels: 37.3 us -> 36.1 us
  local copies, waits for them, and re-layouts: 1.67 us -> 0.71 us
    pallas_call x1, Pallas kernels: 37.3 us -> 36.1 us  [local(): pl.pallas_call(functools.partial(body, n_sp, n_tp), out_shape=pltpu.VMEM(...]
    unnamed x1, local copies, waits for them, and re-layouts: 1.67 us -> 0.71 us
where the time goes in v3:
time: 37 us; the launch traced here: 36.8 us
  Pallas kernels  36.1 us (98%)
  local copies, waits for them, and re-layouts  0.71 us (2%)
    pallas_call x1, Pallas kernels, local(): pl.pallas_call(functools.partial(body, n_sp, n_tp), out_shape=pltpu.VMEM(...  36.1 us

profile of v3, /device:TPU:27, one launch (start us, length us, event | category | flops | bytes accessed | tf_op | source)
XLA Modules:
  0.0 36.8 jit_solution(2482058365348157904)
XLA Ops:
  0.0 36.1 %shard_map.91 = bf16[256,512]{1,0:T(8,128)(2,1)S(1)} custom-call(bf16[256,2048]{1,0:T(8,128)(2,1)} %stream.1, f32[2,2048]{1,0:T(2,128)} %attn_gain_in.1, bf16[2,2048,512]{2,1,0:T(8,128)(2,1)} %w_query.1, bf16[2,2048,128]{2,1,0:T(8,128)(2,1)} %w_key.1, bf16[2,2048,128]{2,1,0:T(8,128)(2,1)} %w_value.1, bf16[2,512,2048]{2,1,0:T(8,128)(2,1)} %w_out.1, ...), custom_call_target="tpu_custom_call" | custom-call | tf_op jit(solution)/shard_map/pallas_call | solution.py:484
  36.1 0.7 %copy.11 = bf16[256,512]{1,0:T(8,128)(2,1)} copy(bf16[256,512]{1,0:T(8,128)(2,1)S(1)} %shard_map.91) | data formatting | bytes 524288

commit v4 on v3

--- a/solution.py
+++ b/solution.py
@@ -274,7 +274,6 @@
     weight_loads[0][2].wait()
     queries[...] = make_queries(0, normed[...])
     build_bias(0)
-    build_bias(1)
     weight_loads[0][3].wait()
 
     def mine_at(i):
@@ -328,6 +327,7 @@
         return carry
 
     lax.fori_loop(0, half, first_out, 0)
+    build_bias(1)
 
     for l in range(1, LAYERS):
         for copy in weight_loads[l]:

time: 37 us -> 37 us (level)
  no operation moved by 1% of the time
where the time goes in v4:
time: 37 us; the launch traced here: 36.8 us
  Pallas kernels  36.1 us (98%)
  local copies, waits for them, and re-layouts  0.71 us (2%)
    pallas_call x1, Pallas kernels, local(): pl.pallas_call(functools.partial(body, n_sp, n_tp), out_shape=pltpu.VMEM(...  36.1 us

profile of v4, /device:TPU:27, one launch (start us, length us, event | category | flops | bytes accessed | tf_op | source)
XLA Modules:
  0.0 36.8 jit_solution(1946438398628161356)
XLA Ops:
  0.0 36.1 %shard_map.91 = bf16[256,512]{1,0:T(8,128)(2,1)S(1)} custom-call(bf16[256,2048]{1,0:T(8,128)(2,1)} %stream.1, f32[2,2048]{1,0:T(2,128)} %attn_gain_in.1, bf16[2,2048,512]{2,1,0:T(8,128)(2,1)} %w_query.1, bf16[2,2048,128]{2,1,0:T(8,128)(2,1)} %w_key.1, bf16[2,2048,128]{2,1,0:T(8,128)(2,1)} %w_value.1, bf16[2,512,2048]{2,1,0:T(8,128)(2,1)} %w_out.1, ...), custom_call_target="tpu_custom_call" | custom-call | tf_op jit(solution)/shard_map/pallas_call | solution.py:484
  36.1 0.7 %copy.11 = bf16[256,512]{1,0:T(8,128)(2,1)} copy(bf16[256,512]{1,0:T(8,128)(2,1)S(1)} %shard_map.91) | data formatting | bytes 524288
